TPU v7x, 32 devices: a whole 2x2x4 slice. The times are simulated.
32 devices in a mesh: sp: 8 (over z, core), tp: 4 (over y, x).
Axes of the slice: x: 2, y: 2, z: 4, core: 2. Of those that a mesh axis runs over, the one named last changes fastest.
Arguments:
- resid: bfloat16 [4096, 2048], P(('sp', 'tp')), may hold values from -6 to 6
- branch_input: bfloat16 [1024, 4096], P('tp', 'sp'), may hold values from -6 to 6
- gate_in: bfloat16 [1024, 4096], P('tp', 'sp'), may hold values from -6 to 6
- conv_taps: bfloat16 [4, 1024], P(None, 'tp'), may hold values from -3 to 3
- rate_weight: bfloat16 [16, 64, 64], P('tp'), may hold values from -0.75 to 0.75
- input_weight: bfloat16 [16, 64, 64], P('tp'), may hold values from -0.75 to 0.75
- decay_base: float32 [1024], P('tp')
- decay_extra: float32 [4096], P('sp'), may hold values from -2 to 0
- out_weight: bfloat16 [1024, 2048], P('tp'), may hold values from -0.1875 to 0.1875
- gain_mix: float32 [2048], replicated, may hold values from 0.1 to 1.9
- gain_pre: float32 [2048], replicated, may hold values from 0.1 to 1.9
- gain_post: float32 [2048], replicated, may hold values from 0.1 to 1.9
- expert_ids: int32 [4096, 2], P(('sp', 'tp')), may hold values from 0 to 7, as said below
- route_weight: float32 [4096, 2], P(('sp', 'tp')), may hold values from 0.2 to 1
- gate_proj: bfloat16 [8, 512, 2048], P('sp', 'tp'), may hold values from -0.125 to 0.125
- up_proj: bfloat16 [8, 512, 2048], P('sp', 'tp'), may hold values from -0.125 to 0.125
- down_proj: bfloat16 [8, 512, 2048], P('sp', 'tp'), may hold values from -0.25 to 0.25
Outputs:
- layer_out: bfloat16 [4096, 2048], P(('sp', 'tp'))
Inputs may be any that keep to these rules, and one draw needn't show every extreme that they name: `expert_ids`: each row names two different experts of one group: both lie in g * 2 .. g * 2 + 1 for some g. In each aligned block of 128 rows (the rows of one device) every expert is named by exactly 32 rows.
All inputs are finite; a program needn't handle non-finite values.
Results may differ from a plain program's by a relative error of at most 0.0065.
Values may be sent and summed in bfloat16 or wider, within the bound.
A program may use at most 128 MiB of HBM per device.

v0:
```python
import math

import jax
import jax.numpy as jnp
from jax import lax
from jax.sharding import PartitionSpec as P

epsilon = 1e-06
gate_power = 8.0


def entering_2(array, axis, combine, identity):
    count, here = (lax.axis_size(axis), lax.axis_index(axis))
    everything = jax.tree.map(lambda part: lax.all_gather(part, axis), array)
    start = jax.tree.map(
        lambda part, zero: jnp.broadcast_to(jnp.asarray(zero, part.dtype), part.shape),
        array,
        identity,
    )

    def hop(k, before):
        reached = k < here
        new = combine(before, jax.tree.map(lambda part: part[k], everything))
        return jax.tree.map(lambda a, b: jnp.where(reached, a, b), new, before)

    return lax.fori_loop(0, count, hop, start)


def passed_along(value, axis, steps):
    count = lax.axis_size(axis)
    first, last = (max(0, -steps), min(count, count - steps))
    return lax.ppermute(value, axis, [(source, source + steps) for source in range(first, last)])


def normalized(values, gain):
    return values * lax.rsqrt(jnp.mean(values * values, axis=-1, keepdims=True) + epsilon) * gain


def combine_pair(earlier, latter):
    return (earlier[0] * latter[0], latter[0] * earlier[1] + latter[1])


def carry_in(block_keep, block_state):
    identity = (jnp.ones(block_keep.shape, jnp.float32), jnp.zeros(block_state.shape, jnp.float32))
    return entering_2((block_keep, block_state), "sp", combine_pair, identity)


def block_cumsum(log_keep):
    channels, positions = log_keep.shape
    span = math.gcd(positions, 128)
    count = positions // span
    shaped = log_keep.reshape(channels, count, span)
    inner = jnp.cumsum(shaped, axis=2)
    before = jnp.cumsum(inner[:, :, -1], axis=1) - inner[:, :, -1]
    return (inner + before[:, :, None]).reshape(channels, positions)


def block_recurrence(log_keep, driven, start_state):
    channels, positions = log_keep.shape
    span = math.gcd(positions, 128)
    count = positions // span
    order = jnp.arange(span, dtype=jnp.int32)
    lower = (order[:, None] >= order[None, :])[None, :, :]

    def one_block(index, carried):
        state, total_log, states_out, logs_out = carried
        first = index * span
        block_log = lax.dynamic_slice_in_dim(log_keep, first, span, 1)
        block_drive = lax.dynamic_slice_in_dim(driven, first, span, 1)
        running = jnp.cumsum(block_log, axis=1)
        gap = jnp.where(lower, running[:, :, None] - running[:, None, :], -jnp.inf)
        inner = jnp.einsum("cts,cs->ct", jnp.exp(gap), block_drive, precision=lax.Precision.HIGHEST)
        produced = inner + jnp.exp(running) * state[:, None]
        whole_log = running + total_log[:, None]
        states_out = lax.dynamic_update_slice_in_dim(states_out, produced, first, 1)
        logs_out = lax.dynamic_update_slice_in_dim(logs_out, whole_log, first, 1)
        return (produced[:, -1], whole_log[:, -1], states_out, logs_out)

    initial = (
        start_state,
        jnp.zeros((channels,), jnp.float32),
        jnp.zeros((channels, positions), jnp.float32),
        jnp.zeros((channels, positions), jnp.float32),
    )
    _, _, hidden_state, summed_log = lax.fori_loop(0, count, one_block, initial)
    return (hidden_state, summed_log)


def per_device(
    resid,
    branch_input,
    gate_in,
    conv_taps,
    rate_weight,
    input_weight,
    decay_base,
    decay_extra,
    out_weight,
    gain_mix,
    gain_pre,
    gain_post,
    expert_ids,
    route_weight,
    gate_proj,
    up_proj,
    down_proj,
):
    channels, positions = branch_input.shape
    tap_count = conv_taps.shape[0]
    edge_cols = passed_along(branch_input[:, positions - (tap_count - 1) :], "sp", 1)
    padded = jnp.concatenate([edge_cols, branch_input], axis=1).astype(jnp.float32)
    filter_tap_weights = conv_taps.astype(jnp.float32)
    convolved = filter_tap_weights[0][:, None] * padded[:, 0:positions]
    for offset in range(1, tap_count):
        convolved = (
            convolved + filter_tap_weights[offset][:, None] * padded[:, offset : offset + positions]
        )
    grouped = convolved.reshape(rate_weight.shape[0], rate_weight.shape[1], positions)
    rate_gate = jax.nn.sigmoid(
        jnp.einsum(
            "ncs,ncd->nds",
            grouped,
            rate_weight.astype(jnp.float32),
            precision=lax.Precision.HIGHEST,
        ).reshape(channels, positions)
    )
    input_gate = jax.nn.sigmoid(
        jnp.einsum(
            "ncs,ncd->nds",
            grouped,
            input_weight.astype(jnp.float32),
            precision=lax.Precision.HIGHEST,
        ).reshape(channels, positions)
    )
    decay_rate = -gate_power * jax.nn.softplus(-decay_base)
    log_keep = decay_rate[:, None] * rate_gate + decay_extra[None, :]
    driven = jnp.sqrt(-jnp.expm1(2.0 * log_keep)) * input_gate * convolved
    summed_log = block_cumsum(log_keep)
    tail_keep = jnp.exp(summed_log[:, -1:] - summed_log)
    _, entering = carry_in(jnp.exp(summed_log[:, -1]), jnp.sum(driven * tail_keep, axis=1))
    hidden_state = block_recurrence(log_keep, driven, entering)[0]
    branch_out = (hidden_state * jax.nn.gelu(gate_in.astype(jnp.float32), approximate=True)).astype(
        jnp.bfloat16
    )
    token_rows = lax.all_to_all(branch_out, "tp", split_axis=1, concat_axis=0, tiled=True)
    token_count = token_rows.shape[1]
    mixed_rows = lax.dot_general(
        token_rows,
        lax.all_gather(out_weight, "tp", axis=0, tiled=True),
        (((0,), (0,)), ((), ())),
        preferred_element_type=jnp.float32,
    )
    after_mix = resid.astype(jnp.float32) + normalized(mixed_rows, gain_mix)
    ffn_in = normalized(after_mix, gain_pre).astype(jnp.bfloat16)
    top_count = expert_ids.shape[1]
    experts = gate_proj.shape[0] * lax.axis_size("sp")
    capacity = top_count * token_count // experts
    chosen = expert_ids.reshape(-1)
    matches = (chosen[:, None] == jnp.arange(experts, dtype=jnp.int32)[None, :]).astype(jnp.int32)
    slot_index = jnp.sum((jnp.cumsum(matches, axis=0) - 1) * matches, axis=1)
    target = chosen * capacity + slot_index
    source = (
        jnp.zeros((experts * capacity,), jnp.int32)
        .at[target]
        .set(jnp.arange(token_count * top_count, dtype=jnp.int32) // top_count)
    )
    outgoing = ffn_in[source].reshape(experts, capacity, ffn_in.shape[1])
    arriving = lax.all_to_all(outgoing, "sp", split_axis=0, concat_axis=1, tiled=True)
    gate_rows = lax.all_gather(gate_proj, "tp", axis=1, tiled=True)
    up_rows = lax.all_gather(up_proj, "tp", axis=1, tiled=True)
    down_rows = lax.all_gather(down_proj, "tp", axis=1, tiled=True)
    gate_vals = jnp.einsum("emd,ekd->emk", arriving, gate_rows, preferred_element_type=jnp.float32)
    up_vals = jnp.einsum("emd,ekd->emk", arriving, up_rows, preferred_element_type=jnp.float32)
    hidden = (jax.nn.silu(gate_vals) * up_vals).astype(jnp.bfloat16)
    result = jnp.einsum("emk,ekd->emd", hidden, down_rows, preferred_element_type=jnp.float32)
    returned = lax.all_to_all(
        result.astype(jnp.bfloat16), "sp", split_axis=1, concat_axis=0, tiled=True
    )
    returned = returned.reshape(experts * capacity, returned.shape[2])
    picked = returned[target].astype(jnp.float32).reshape(token_count, top_count, returned.shape[1])
    moe = jnp.sum(picked * route_weight[:, :, None], axis=1)
    return (after_mix + normalized(moe, gain_post)).astype(jnp.bfloat16)


def solution(mesh):
    in_specs = (
        P(("sp", "tp"), None),
        P("tp", "sp"),
        P("tp", "sp"),
        P(None, "tp"),
        P("tp", None, None),
        P("tp", None, None),
        P("tp"),
        P("sp"),
        P("tp", None),
        P(),
        P(),
        P(),
        P(("sp", "tp"), None),
        P(("sp", "tp"), None),
        P("sp", "tp", None),
        P("sp", "tp", None),
        P("sp", "tp", None),
    )
    out_specs = P(("sp", "tp"), None)
    return jax.shard_map(
        per_device, mesh=mesh, in_specs=in_specs, out_specs=out_specs, check_vma=False
    )
```

profile of v0, /device:TPU:0, one launch (start us, length us, event | category | flops | bytes accessed | tf_op | source)
XLA Modules:
  0.0 288.3 jit_solution(16945330147929977153)
XLA Ops:
  7.3 0.7 all-gather.10.cloned.1.call-update
  8.9 2.4 collective-permute-start
  13.2 1.4 scatter_custom_fusion
  17.7 0.9 multiply_reduce_fusion.4
  18.6 13.4 %all-gather.2 = f32[8,1,256]{2,1,0:T(1,128)S(1)} all-gather(f32[1,1,256]{2,1,0:T(1,128)S(1)} %bitcast.139), channel_id=3, replica_groups=mesh['sp'=8,'tp'=4] {'sp'}, dimensions={0}, use_global_device_ids=true | all-gather | bytes 9216 | tf_op jit(solution)/shard_map/all_gather | solution.py:14
  32.0 8.7 %all-gather = f32[2048,1]{0,1:T(1,128)S(1)} all-gather(f32[256,1]{0,1:T(1,128)S(1)} %get-tuple-element.288), channel_id=2, replica_groups=mesh['sp'=8,'tp'=4] {'sp'}, dimensions={0}, use_global_device_ids=true | all-gather | bytes 9216 | tf_op jit(solution)/shard_map/all_gather | solution.py:14
  41.3 0.7 reduce.5
  42.5 126.3 %while.30 = (s32[]{:T(128)}, f32[256]{0:T(256)S(1)}, f32[256,512]{1,0:T(8,128)S(1)}, f32[256,512]{1,0:T(8,128)S(1)}, f32[256,512]{1,0:T(8,128)S(1)}, /*index=5*/...) while((s32[]{:T(128)}, f32[256]{0:T(256)S(1)}, f32[256,512]{1,0:T(8,128)S(1)}, ...), condition=%wide.region_7.8_spmd.clone, body=%wide.region_5.7_spmd.clone.sunk | while | flops 62963716 | bytes 2919583 | solution.py:85
  57.0 27.2 %fusion.83 = f32[256,1,128]{2,1,0:T(1,128)S(1)} fusion(f32[256,128,1]{1,2,0:T(1,128)S(1)} %bitcast.110, f32[256,128]{1,0:T(8,128)S(1)} %copy.123, pred[128,128]{1,0:T(8,128)(4,1)S(1)} %fusion.82), kind=kOutput, calls=%fused_computation.4.clone.1 | convolution fusion | flops 58720256 | bytes 409600 | tf_op jit(solution)/shard_map/while/body/eval_jaxpr/cts,cs->ct/dot_general | solution.py:72
  85.0 27.2 %fusion.83 = f32[256,1,128]{2,1,0:T(1,128)S(1)} fusion(f32[256,128,1]{1,2,0:T(1,128)S(1)} %bitcast.110, f32[256,128]{1,0:T(8,128)S(1)} %copy.123, pred[128,128]{1,0:T(8,128)(4,1)S(1)} %fusion.82), kind=kOutput, calls=%fused_computation.4.clone.1 | convolution fusion | flops 58720256 | bytes 409600 | tf_op jit(solution)/shard_map/while/body/eval_jaxpr/cts,cs->ct/dot_general | solution.py:72
  113.0 27.2 %fusion.83 = f32[256,1,128]{2,1,0:T(1,128)S(1)} fusion(f32[256,128,1]{1,2,0:T(1,128)S(1)} %bitcast.110, f32[256,128]{1,0:T(8,128)S(1)} %copy.123, pred[128,128]{1,0:T(8,128)(4,1)S(1)} %fusion.82), kind=kOutput, calls=%fused_computation.4.clone.1 | convolution fusion | flops 58720256 | bytes 409600 | tf_op jit(solution)/shard_map/while/body/eval_jaxpr/cts,cs->ct/dot_general | solution.py:72
  141.0 27.2 %fusion.83 = f32[256,1,128]{2,1,0:T(1,128)S(1)} fusion(f32[256,128,1]{1,2,0:T(1,128)S(1)} %bitcast.110, f32[256,128]{1,0:T(8,128)S(1)} %copy.123, pred[128,128]{1,0:T(8,128)(4,1)S(1)} %fusion.82), kind=kOutput, calls=%fused_computation.4.clone.1 | convolution fusion | flops 58720256 | bytes 409600 | tf_op jit(solution)/shard_map/while/body/eval_jaxpr/cts,cs->ct/dot_general | solution.py:72
  168.8 0.9 copy_bitcast_fusion.1
  169.7 3.7 %all-to-all-start = ((bf16[256,4,128]{2,0,1:T(8,128)(2,1)}), bf16[256,4,128]{2,0,1:T(8,128)(2,1)S(1)}, u32[]{:S(2)}, u32[]{:S(2)}) async-start(bf16[256,4,128]{2,0,1:T(8,128)(2,1)} %copy_bitcast_fusion.1), calls=%async_computation | async-start | bytes 524288 | tf_op jit(solution)/shard_map/all_to_all | solution.py:145
  173.4 5.9 %all-to-all-done = bf16[256,4,128]{2,0,1:T(8,128)(2,1)S(1)} async-done(((bf16[256,4,128]{2,0,1:T(8,128)(2,1)}), bf16[256,4,128]{2,0,1:T(8,128)(2,1)S(1)}, u32[]{:S(2)}, u32[]{:S(2)}) %all-to-all-start) | async-done | bytes 262176 | tf_op jit(solution)/shard_map/all_to_all | solution.py:145
  179.3 3.1 %multiply_reduce_fusion.3 = (f32[128]{0:T(128)S(1)}, f32[128,2048]{1,0:T(8,128)S(1)}) fusion(bf16[1024,128]{1,0:T(8,128)(2,1)S(1)} %bitcast.116, bf16[1024,2048]{1,0:T(8,128)(2,1)} %all-gather.8.cloned.1.call-done), kind=kOutput, calls=%fused_computation.46 | convolution fusion | flops 537395072 | bytes 5505536 | tf_op jit(solution)/shard_map/dot_general | solution.py:147
  183.1 2.3 gather_fusion
  185.4 3.6 %all-to-all-start.1 = ((bf16[8,32,2048]{2,1,0:T(8,128)(2,1)}), bf16[8,32,2048]{2,1,0:T(8,128)(2,1)S(1)}, u32[]{:S(2)}, u32[]{:S(2)}) async-start(bf16[8,32,2048]{2,1,0:T(8,128)(2,1)} %bitcast.20), calls=%async_computation.1 | async-start | bytes 2097152 | tf_op jit(solution)/shard_map/all_to_all | solution.py:168
  189.0 26.5 %all-to-all-done.1 = bf16[8,32,2048]{2,1,0:T(8,128)(2,1)S(1)} async-done(((bf16[8,32,2048]{2,1,0:T(8,128)(2,1)}), bf16[8,32,2048]{2,1,0:T(8,128)(2,1)S(1)}, u32[]{:S(2)}, u32[]{:S(2)}) %all-to-all-start.1) | async-done | bytes 1048608 | tf_op jit(solution)/shard_map/all_to_all | solution.py:168
  215.5 2.3 fusion.16
  217.9 4.6 %fusion.12 = bf16[1,256,2048]{2,1,0:T(8,128)(2,1)} fusion(bf16[1,512,2048]{2,1,0:T(8,128)(2,1)} %all-gather.14.cloned.1.call-done, bf16[256,2048]{1,0:T(8,128)(2,1)S(1)} %bitcast.118, bf16[1,512,2048]{2,1,0:T(8,128)(2,1)} %all-gather.12.cloned.1.call-done, f32[256,512]{1,0:T(8,128)S(1)} %fusion.16), kind=kOutput, calls=%fused_computation.23 | convolution fusion | flops 1075052544 | bytes 6815744 | tf_op jit(solution)/shard_map/emk,ekd->emd/dot_general | solution.py:175
  222.5 2.8 copy.117
  225.8 7.8 %reduce.6 = bf16[256,2048]{1,0:T(8,128)(2,1)} reduce(bf16[256,1,2048]{2,1,0:T(2,128)(2,1)S(1)} %bitcast.109, bf16[]{:T(256)} %broadcast.210), dimensions={1}, to_apply=%bitcast.89.reduce_sub_computation | reduce | bytes 2097154
  233.6 2.6 reshape.255
  236.3 3.8 %all-to-all-start.2 = ((bf16[8,2,32768]{2,1,0:T(2,128)(2,1)}), bf16[8,2,32768]{2,1,0:T(2,128)(2,1)S(1)}, u32[]{:S(2)}, u32[]{:S(2)}) async-start(bf16[8,2,32768]{2,1,0:T(2,128)(2,1)} %reshape.255), calls=%async_computation.2 | async-start | bytes 2097152 | tf_op jit(solution)/shard_map/all_to_all | solution.py:176
  240.2 26.3 %all-to-all-done.2 = bf16[8,2,32768]{2,1,0:T(2,128)(2,1)S(1)} async-done(((bf16[8,2,32768]{2,1,0:T(2,128)(2,1)}), bf16[8,2,32768]{2,1,0:T(2,128)(2,1)S(1)}, u32[]{:S(2)}, u32[]{:S(2)}) %all-to-all-start.2) | async-done | bytes 1048608 | tf_op jit(solution)/shard_map/all_to_all | solution.py:176
  266.5 3.5 %reshape.256 = bf16[256,1,2048]{2,1,0:T(2,128)(2,1)} reshape(bf16[8,2,32768]{2,1,0:T(2,128)(2,1)S(1)} %all-to-all-done.2) | data formatting | bytes 2097152
  270.0 2.2 copy.115
  272.2 2.3 gather_fusion.1
  274.5 2.4 reshape.210
  276.9 3.2 %multiply_reduce_fusion = f32[128,2048]{1,0:T(8,128)S(1)} fusion(f32[128,2,2048]{2,1,0:T(2,128)S(1)} %reshape.210, f32[128,2]{1,0:T(8,128)S(1)} %copy.93), kind=kLoop, calls=%fused_computation.29 | loop fusion | flops 786432 | bytes 3146752 | tf_op jit(solution)/shard_map/reduce_sum | solution.py:181
  280.3 1.2 add_convert_fusion
  (146 shorter events, 11.9 us)
Async XLA Ops:
  6.5 8.9 %copy-start = (bf16[4,64,64]{2,1,0:T(8,128)(2,1)S(1)}, bf16[4,64,64]{2,1,0:T(8,128)(2,1)}, u32[]{:S(2)}) copy-start(bf16[4,64,64]{2,1,0:T(8,128)(2,1)} %param.25) | copy-start | bytes 98308
  6.5 2.3 copy-start.3
  6.5 4.8 %copy-start.10 = (s32[128,2]{0,1:T(2,128)S(1)}, s32[128,2]{0,1:T(2,128)}, u32[]{:S(2)}) copy-start(s32[128,2]{0,1:T(2,128)} %param.33) | copy-start | bytes 3076
  6.5 5.2 %copy-start.9 = (bf16[4,256]{1,0:T(4,128)(2,1)S(1)}, bf16[4,256]{1,0:T(4,128)(2,1)}, u32[]{:S(2)}) copy-start(bf16[4,256]{1,0:T(4,128)(2,1)} %param.24) | copy-start | bytes 6148
  6.5 5.3 %copy-start.12 = (f32[256]{0:T(256)S(1)}, f32[256]{0:T(256)}, u32[]{:S(2)}) copy-start(f32[256]{0:T(256)} %param.27) | copy-start | bytes 3076
  6.5 6.5 %copy-start.8 = (f32[512]{0:T(512)S(1)}, f32[512]{0:T(512)}, u32[]{:S(2)}) copy-start(f32[512]{0:T(512)} %param.28) | copy-start | bytes 6148
  6.6 172.7 %all-gather.8.cloned.1.call-start = ((), (), s32[]{:S(2)}) async-start(), calls=%async_computation.3 | async-start | bytes 5242880 | tf_op jit(solution)/shard_map/all_gather | solution.py:149
  7.3 181.7 %all-gather.10.cloned.1.call-start = ((), (), s32[]{:S(2)}) async-start(), calls=%async_computation.4 | async-start | bytes 2621440 | tf_op jit(solution)/shard_map/all_gather | solution.py:169
  8.0 209.8 %all-gather.12.cloned.1.call-start = ((), (), s32[]{:S(2)}) async-start(), calls=%async_computation.5 | async-start | bytes 2621440 | tf_op jit(solution)/shard_map/all_gather | solution.py:170
  8.8 209.1 %all-gather.14.cloned.1.call-start = ((), (), s32[]{:S(2)}) async-start(), calls=%async_computation.6 | async-start | bytes 2621440 | tf_op jit(solution)/shard_map/all_gather | solution.py:171
  8.9 5.7 %collective-permute-start = (bf16[256,3]{1,0:T(8,128)(2,1)S(1)}, bf16[256,3]{1,0:T(8,128)(2,1)S(1)}, u32[]{:S(2)}, u32[]{:S(2)}) collective-permute-start(bf16[256,3]{1,0:T(8,128)(2,1)S(1)} %slice.49), channel_id=1, source_target_pairs={{0,4},{4,8},{8,12},{12,16},{16,20},{20,24},{24,28},{1,5},{5,9},{9,... | collective-permute-start | bytes 4616 | tf_op jit(solution)/shard_map/ppermute | solution.py:32
  16.3 0.8 copy-start.13
  42.5 126.3 %copy-start.4 = (bf16[256,512]{1,0:T(8,128)(2,1)S(1)}, bf16[256,512]{1,0:T(8,128)(2,1)}, u32[]{:S(2)}) copy-start(bf16[256,512]{1,0:T(8,128)(2,1)} %param.23) | copy-start | bytes 786436
  169.7 9.6 %all-to-all-start = ((bf16[256,4,128]{2,0,1:T(8,128)(2,1)}), bf16[256,4,128]{2,0,1:T(8,128)(2,1)S(1)}, u32[]{:S(2)}, u32[]{:S(2)}) async-start(bf16[256,4,128]{2,0,1:T(8,128)(2,1)} %copy_bitcast_fusion.1), calls=%async_computation | async-start | bytes 524288 | tf_op jit(solution)/shard_map/all_to_all | solution.py:145
  179.3 3.1 %copy-start.1 = (bf16[128,2048]{1,0:T(8,128)(2,1)S(1)}, bf16[128,2048]{1,0:T(8,128)(2,1)}, u32[]{:S(2)}) copy-start(bf16[128,2048]{1,0:T(8,128)(2,1)} %param.21) | copy-start | bytes 1572868
  179.3 3.1 %copy-start.5 = (f32[2048]{0:T(1024)S(1)}, f32[2048]{0:T(1024)}, u32[]{:S(2)}) copy-start(f32[2048]{0:T(1024)} %param.30) | copy-start | bytes 24580
  179.3 3.5 %copy-start.6 = (f32[2048]{0:T(1024)S(1)}, f32[2048]{0:T(1024)}, u32[]{:S(2)}) copy-start(f32[2048]{0:T(1024)} %param.31) | copy-start | bytes 24580
  185.4 30.1 %all-to-all-start.1 = ((bf16[8,32,2048]{2,1,0:T(8,128)(2,1)}), bf16[8,32,2048]{2,1,0:T(8,128)(2,1)S(1)}, u32[]{:S(2)}, u32[]{:S(2)}) async-start(bf16[8,32,2048]{2,1,0:T(8,128)(2,1)} %bitcast.20), calls=%async_computation.1 | async-start | bytes 2097152 | tf_op jit(solution)/shard_map/all_to_all | solution.py:168
  233.6 6.4 %copy-start.11 = (f32[128,2]{0,1:T(2,128)S(1)}, f32[128,2]{0,1:T(2,128)}, u32[]{:S(2)}) copy-start(f32[128,2]{0,1:T(2,128)} %param.34) | copy-start | bytes 3076
  236.3 30.3 %all-to-all-start.2 = ((bf16[8,2,32768]{2,1,0:T(2,128)(2,1)}), bf16[8,2,32768]{2,1,0:T(2,128)(2,1)S(1)}, u32[]{:S(2)}, u32[]{:S(2)}) async-start(bf16[8,2,32768]{2,1,0:T(2,128)(2,1)} %reshape.255), calls=%async_computation.2 | async-start | bytes 2097152 | tf_op jit(solution)/shard_map/all_to_all | solution.py:176
  276.9 3.4 %copy-start.2 = (bf16[128,2048]{1,0:T(8,128)(2,1)S(1)}, bf16[128,2048]{1,0:T(8,128)(2,1)}, u32[]{:S(2)}) copy-start(bf16[128,2048]{1,0:T(8,128)(2,1)} %param.21) | copy-start | bytes 1572868
  276.9 3.4 %copy-start.7 = (f32[2048]{0:T(1024)S(1)}, f32[2048]{0:T(1024)}, u32[]{:S(2)}) copy-start(f32[2048]{0:T(1024)} %param.32) | copy-start | bytes 24580
Sparse Core Ops, SparseCore 0:
  9.2 55.2 all-gather.7
  66.4 35.1 all-gather.9
  103.4 35.1 all-gather.11
  140.4 35.1 all-gather.13
where the time goes:
time: 293 us; the launch traced here: 288 us
  matrix products  120 us (41%)
  waiting for transfers between devices  60.8 us (21%)
  local copies, waits for them, and re-layouts  24.8 us (8%)
  blocking collectives  22.1 us (8%)
  other arithmetic  18.4 us (6%)
  loops' own time  14.9 us (5%)
  between operations  13.8 us (5%)
  starting transfers between devices  13.6 us (5%)
    dot_general x4, matrix products, one_block(): jnp.einsum('cts,cs->ct', jnp.exp(gap), block_drive, precision=lax.Precisi...  109 us
    all_to_all x1, waiting for transfers between devices, per_device(): lax.all_to_all(outgoing, 'sp', split_axis=0, concat_axis=1, tiled=True)  26.5 us
    all_to_all x1, waiting for transfers between devices, per_device(): lax.all_to_all(result.astype(jnp.bfloat16), 'sp', split_axis=1, concat_ax...  26.3 us
    all_gather x2, blocking collectives, entering_2(): everything = jax.tree.map(lambda part: lax.all_gather(part, axis), array)  22.1 us
    another operation x1, loops' own time, block_recurrence(): _, _, hidden_state, summed_log = lax.fori_loop(0, count, one_block, initial)  14.7 us
    unnamed x36, local copies, waits for them, and re-layouts  9.28 us
    unnamed x2, other arithmetic  7.79 us
  transfers between devices with their start and end apart: 8, of which 3 were waited for; matrix products, arithmetic and copies ran while one was open for 45% of the time, Pallas kernels for 0%

commit v1 on v0

v1 whole, which is shorter than its diff:
```python
import jax
import jax.numpy as jnp
from jax import lax
from jax.experimental import pallas as pl
from jax.experimental.pallas import tpu as pltpu
from jax.sharding import PartitionSpec as P

epsilon = 1e-06
gate_power = 8.0


def entering_2(array, axis, combine, identity):
    count, here = (lax.axis_size(axis), lax.axis_index(axis))
    everything = jax.tree.map(lambda part: lax.all_gather(part, axis), array)
    start = jax.tree.map(
        lambda part, zero: jnp.broadcast_to(jnp.asarray(zero, part.dtype), part.shape),
        array,
        identity,
    )

    def hop(k, before):
        reached = k < here
        new = combine(before, jax.tree.map(lambda part: part[k], everything))
        return jax.tree.map(lambda a, b: jnp.where(reached, a, b), new, before)

    return lax.fori_loop(0, count, hop, start)


def passed_along(value, axis, steps):
    count = lax.axis_size(axis)
    first, last = (max(0, -steps), min(count, count - steps))
    return lax.ppermute(value, axis, [(source, source + steps) for source in range(first, last)])


def normalized(values, gain):
    return values * lax.rsqrt(jnp.mean(values * values, axis=-1, keepdims=True) + epsilon) * gain


def combine_pair(earlier, latter):
    return (earlier[0] * latter[0], latter[0] * earlier[1] + latter[1])


def carry_in(block_keep, block_state):
    identity = (jnp.ones(block_keep.shape, jnp.float32), jnp.zeros(block_state.shape, jnp.float32))
    return entering_2((block_keep, block_state), "sp", combine_pair, identity)


def shifted(values, fill, distance, lane):
    return jnp.where(lane >= distance, pltpu.roll(values, distance, 1), fill)


def one_minus_exp(y):
    small = 1.0 + y * (1.0 / 8.0)
    for k in range(7, 1, -1):
        small = 1.0 + y * (1.0 / k) * small
    return jnp.where(y > -0.5, -y * small, 1.0 - jnp.exp(y))


def split_three(values):
    high = values.astype(jnp.bfloat16)
    rest = values - high.astype(jnp.float32)
    mid = rest.astype(jnp.bfloat16)
    low = (rest - mid.astype(jnp.float32)).astype(jnp.bfloat16)
    return high, mid, low


def scan_kernel(edge_ref, input_ref, taps_ref, rate_ref, inward_ref, decay_ref, extra_ref, keep_ref, state_ref):
    taps = taps_ref[0]
    positions = input_ref.shape[1]
    here = input_ref[...].astype(jnp.float32)
    padded = jnp.concatenate([edge_ref[...].astype(jnp.float32), here], axis=1)
    pad = padded.shape[1] - positions
    count = taps.shape[1]
    convolved = taps[:, count - 1 : count] * here
    for back in range(1, count):
        moved = pltpu.roll(padded, back, 1)[:, pad:]
        convolved = convolved + taps[:, count - 1 - back : count - back] * moved
    stacked = jnp.concatenate(split_three(convolved), axis=0)

    def gate(weight):
        return jax.nn.sigmoid(
            lax.dot_general(
                jnp.concatenate([weight] * 3, axis=0),
                stacked,
                (((0,), (0,)), ((), ())),
                preferred_element_type=jnp.float32,
            )
        )

    log_keep = decay_ref[0] * gate(rate_ref[0]) + extra_ref[...]
    state = jnp.sqrt(one_minus_exp(2.0 * log_keep)) * gate(inward_ref[0]) * convolved
    keep = jnp.exp(log_keep)
    lane = lax.broadcasted_iota(jnp.int32, keep.shape, 1)
    distance = 1
    while distance < positions:
        state = keep * shifted(state, 0.0, distance, lane) + state
        keep = keep * shifted(keep, 1.0, distance, lane)
        distance *= 2
    keep_ref[...] = keep
    state_ref[...] = state


def local_scan(edge, branch_input, conv_taps, rate_weight, input_weight, decay_rate, decay_extra):
    channels, positions = branch_input.shape
    blocks, width = rate_weight.shape[:2]
    taps = conv_taps.astype(jnp.float32).T.reshape(blocks, width, conv_taps.shape[0])
    pad = 128
    edge = jnp.pad(edge, ((0, 0), (pad - edge.shape[1], 0)))
    row = lambda i: (i, 0)
    block3 = lambda i: (i, 0, 0)
    return pl.pallas_call(
        scan_kernel,
        grid=(blocks,),
        in_specs=[
            pl.BlockSpec((width, pad), row),
            pl.BlockSpec((width, positions), row),
            pl.BlockSpec((1, width, taps.shape[2]), block3),
            pl.BlockSpec((1, width, width), block3),
            pl.BlockSpec((1, width, width), block3),
            pl.BlockSpec((1, width, 1), block3),
            pl.BlockSpec((1, positions), lambda i: (0, 0)),
        ],
        out_specs=[pl.BlockSpec((width, positions), row)] * 2,
        out_shape=[jax.ShapeDtypeStruct((channels, positions), jnp.float32)] * 2,
        cost_estimate=pl.CostEstimate(flops=channels * positions * 400, bytes_accessed=channels * positions * 12, transcendentals=channels * positions * 5),
    )(
        edge,
        branch_input,
        taps,
        rate_weight,
        input_weight,
        decay_rate.reshape(blocks, width, 1),
        decay_extra.reshape(1, positions),
    )


def expert_mlp(rows, gate_rows, up_rows, down_rows):
    contract = (((1,), (1,)), ((), ()))
    gate_vals = lax.dot_general(rows, gate_rows, contract, preferred_element_type=jnp.float32)
    up_vals = lax.dot_general(rows, up_rows, contract, preferred_element_type=jnp.float32)
    hidden = (jax.nn.silu(gate_vals) * up_vals).astype(jnp.bfloat16)
    return jnp.dot(hidden, down_rows, preferred_element_type=jnp.float32).astype(jnp.bfloat16)


def paired_moe(ffn_in, expert_ids, route_weight, gate_rows, up_rows, down_rows):
    tokens, width = ffn_in.shape
    devices = lax.axis_size("sp")
    groups = devices // 2
    cap = tokens // groups
    group = expert_ids[:, 0] // 2
    member = (group[:, None] == jnp.arange(groups, dtype=jnp.int32)[None, :]).astype(jnp.int32)
    slot = group * cap + jnp.sum((jnp.cumsum(member, axis=0) - 1) * member, axis=1)
    place = (slot[None, :] == jnp.arange(tokens, dtype=jnp.int32)[:, None]).astype(jnp.bfloat16)
    even = (expert_ids[:, 0] % 2 == 0)[:, None]
    by_expert = jnp.where(even, route_weight, route_weight[:, ::-1])
    extra = jnp.concatenate(split_three(by_expert), axis=1)
    extra = jnp.pad(extra, ((0, 0), (0, 128 - extra.shape[1])))
    outgoing = jnp.dot(place, jnp.concatenate([ffn_in, extra], axis=1), preferred_element_type=jnp.float32)
    outgoing = outgoing.astype(jnp.bfloat16)
    swap = [(i, i ^ 1) for i in range(devices)]
    mine = lax.all_to_all(outgoing, "sp", split_axis=0, concat_axis=0, tiled=True)
    rows = mine[:, :width]
    other_rows = lax.ppermute(rows, "sp", swap)
    other_out = expert_mlp(other_rows, gate_rows, up_rows, down_rows)
    from_other = lax.ppermute(other_out, "sp", swap)
    own_out = expert_mlp(rows, gate_rows, up_rows, down_rows)
    scale = mine[:, width : width + 6].astype(jnp.float32)
    scale = scale[:, 0:2] + scale[:, 2:4] + scale[:, 4:6]
    first = lax.axis_index("sp") % 2 == 0
    own_scale = jnp.where(first, scale[:, 0:1], scale[:, 1:2])
    other_scale = jnp.where(first, scale[:, 1:2], scale[:, 0:1])
    summed = own_scale * own_out.astype(jnp.float32) + other_scale * from_other.astype(jnp.float32)
    returned = lax.all_to_all(summed.astype(jnp.bfloat16), "sp", split_axis=0, concat_axis=0, tiled=True)
    return lax.dot_general(place, returned, (((0,), (0,)), ((), ())), preferred_element_type=jnp.float32)


def general_moe(ffn_in, expert_ids, route_weight, gate_rows, up_rows, down_rows):
    token_count = ffn_in.shape[0]
    top_count = expert_ids.shape[1]
    experts = gate_rows.shape[0] * lax.axis_size("sp")
    capacity = top_count * token_count // experts
    chosen = expert_ids.reshape(-1)
    matches = (chosen[:, None] == jnp.arange(experts, dtype=jnp.int32)[None, :]).astype(jnp.int32)
    slot_index = jnp.sum((jnp.cumsum(matches, axis=0) - 1) * matches, axis=1)
    target = chosen * capacity + slot_index
    source = (
        jnp.zeros((experts * capacity,), jnp.int32)
        .at[target]
        .set(jnp.arange(token_count * top_count, dtype=jnp.int32) // top_count)
    )
    outgoing = ffn_in[source].reshape(experts, capacity, ffn_in.shape[1])
    arriving = lax.all_to_all(outgoing, "sp", split_axis=0, concat_axis=1, tiled=True)
    gate_vals = jnp.einsum("emd,ekd->emk", arriving, gate_rows, preferred_element_type=jnp.float32)
    up_vals = jnp.einsum("emd,ekd->emk", arriving, up_rows, preferred_element_type=jnp.float32)
    hidden = (jax.nn.silu(gate_vals) * up_vals).astype(jnp.bfloat16)
    result = jnp.einsum("emk,ekd->emd", hidden, down_rows, preferred_element_type=jnp.float32)
    returned = lax.all_to_all(
        result.astype(jnp.bfloat16), "sp", split_axis=1, concat_axis=0, tiled=True
    )
    returned = returned.reshape(experts * capacity, returned.shape[2])
    picked = returned[target].astype(jnp.float32).reshape(token_count, top_count, returned.shape[1])
    return jnp.sum(picked * route_weight[:, :, None], axis=1)


expert_groups = 4


def per_device(
    resid,
    branch_input,
    gate_in,
    conv_taps,
    rate_weight,
    input_weight,
    decay_base,
    decay_extra,
    out_weight,
    gain_mix,
    gain_pre,
    gain_post,
    expert_ids,
    route_weight,
    gate_proj,
    up_proj,
    down_proj,
):
    channels, positions = branch_input.shape
    tap_count = conv_taps.shape[0]
    edge_cols = passed_along(branch_input[:, positions - (tap_count - 1) :], "sp", 1)
    decay_rate = -gate_power * jax.nn.softplus(-decay_base)
    keep, state = local_scan(
        edge_cols, branch_input, conv_taps, rate_weight, input_weight, decay_rate, decay_extra
    )
    _, entering = carry_in(keep[:, -1], state[:, -1])
    hidden_state = state + keep * entering[:, None]
    branch_out = (hidden_state * jax.nn.gelu(gate_in.astype(jnp.float32), approximate=True)).astype(
        jnp.bfloat16
    )
    token_rows = lax.all_to_all(branch_out, "tp", split_axis=1, concat_axis=0, tiled=True)
    token_count = token_rows.shape[1]
    mixed_rows = lax.dot_general(
        token_rows,
        lax.all_gather(out_weight, "tp", axis=0, tiled=True),
        (((0,), (0,)), ((), ())),
        preferred_element_type=jnp.float32,
    )
    after_mix = resid.astype(jnp.float32) + normalized(mixed_rows, gain_mix)
    ffn_in = normalized(after_mix, gain_pre).astype(jnp.bfloat16)
    gate_rows = lax.all_gather(gate_proj, "tp", axis=1, tiled=True)
    up_rows = lax.all_gather(up_proj, "tp", axis=1, tiled=True)
    down_rows = lax.all_gather(down_proj, "tp", axis=1, tiled=True)
    experts = gate_proj.shape[0] * lax.axis_size("sp")
    if gate_proj.shape[0] == 1 and experts // expert_groups == 2:
        moe = paired_moe(ffn_in, expert_ids, route_weight, gate_rows[0], up_rows[0], down_rows[0])
    else:
        moe = general_moe(ffn_in, expert_ids, route_weight, gate_rows, up_rows, down_rows)
    return (after_mix + normalized(moe, gain_post)).astype(jnp.bfloat16)


def solution(mesh):
    in_specs = (
        P(("sp", "tp"), None),
        P("tp", "sp"),
        P("tp", "sp"),
        P(None, "tp"),
        P("tp", None, None),
        P("tp", None, None),
        P("tp"),
        P("sp"),
        P("tp", None),
        P(),
        P(),
        P(),
        P(("sp", "tp"), None),
        P(("sp", "tp"), None),
        P("sp", "tp", None),
        P("sp", "tp", None),
        P("sp", "tp", None),
    )
    out_specs = P(("sp", "tp"), None)
    return jax.shard_map(
        per_device, mesh=mesh, in_specs=in_specs, out_specs=out_specs, check_vma=False
    )
```

time: 293 us -> 216 us (0.74); the launches traced: 288 us -> 215 us
  matrix products: 120 us -> 16.6 us
  blocking collectives: 22.1 us -> 76.8 us
  waiting for transfers between devices: 60.8 us -> 85.4 us
  local copies, waits for them, and re-layouts: 24.8 us -> 5.55 us
  loops' own time: 14.9 us -> 0.25 us
  other arithmetic: 18.4 us -> 4.45 us
  starting transfers between devices: 13.6 us -> 6.34 us
  Pallas kernels: 0 us -> 6.19 us
    dot_general x8 -> x6, matrix products: 117 us -> 13.6 us  [the longest x2 8.35 us: expert_mlp(): jnp.dot(hidden, down_rows, preferred_element_type=jnp.float32)]
    all_to_all x2 -> x0, waiting for transfers between devices: 52.8 us -> none  [the longest x1 26.5 us: per_device(): lax.all_to_all(outgoing, 'sp', split_axis=0, concat_axis=1, tiled=True)]
    all_to_all x0 -> x2, blocking collectives: none -> 40.8 us  [the longest x1 20.8 us: paired_moe(): lax.all_to_all(outgoing, 'sp', split_axis=0, concat_axis=0, tiled=True)]
    all_gather x1, waiting for transfers between devices: 0.02 us -> 36.9 us  [per_device(): gate_rows = lax.all_gather(gate_proj, 'tp', axis=1, tiled=True)]
    all_gather x1, waiting for transfers between devices: 0.02 us -> 34.4 us  [per_device(): down_rows = lax.all_gather(down_proj, 'tp', axis=1, tiled=True)]
    another operation x1 -> x0, loops' own time: 14.7 us -> none  [block_recurrence(): _, _, hidden_state, summed_log = lax.fori_loop(0, count, one_block, initial)]
    all_gather x2, blocking collectives: 22.1 us -> 36.1 us  [entering_2(): everything = jax.tree.map(lambda part: lax.all_gather(part, axis), array)]
    unnamed x36 -> x32, local copies, waits for them, and re-layouts: 9.28 us -> 0.85 us
  transfers between devices with their start and end apart: 8 -> 8, of which waited for: 3 -> 4; matrix products, arithmetic and copies ran while one was open for 45% -> 7% of each run, Pallas kernels for 0% -> 3%
where the time goes in v1:
time: 216 us; the launch traced here: 215 us
  waiting for transfers between devices  85.4 us (40%)
  blocking collectives  76.8 us (36%)
  matrix products  16.6 us (8%)
  between operations  13.5 us (6%)
  starting transfers between devices  6.34 us (3%)
  Pallas kernels  6.19 us (3%)
  local copies, waits for them, and re-layouts  5.55 us (3%)
  other arithmetic  4.45 us (2%)
    all_gather x1, waiting for transfers between devices, per_device(): gate_rows = lax.all_gather(gate_proj, 'tp', axis=1, tiled=True)  36.9 us
    all_gather x2, blocking collectives, entering_2(): everything = jax.tree.map(lambda part: lax.all_gather(part, axis), array)  36.1 us
    all_gather x1, waiting for transfers between devices, per_device(): down_rows = lax.all_gather(down_proj, 'tp', axis=1, tiled=True)  34.4 us
    all_to_all x1, blocking collectives, paired_moe(): lax.all_to_all(outgoing, 'sp', split_axis=0, concat_axis=0, tiled=True)  20.8 us
    all_to_all x1, blocking collectives, paired_moe(): lax.all_to_all(summed.astype(jnp.bfloat16), 'sp', split_axis=0, concat_ax...  20 us
    dot_general x2, matrix products, expert_mlp(): jnp.dot(hidden, down_rows, preferred_element_type=jnp.float32)  8.35 us
    pallas_call x1, Pallas kernels, local_scan(): pl.pallas_call(scan_kernel, grid=(blocks,), in_specs=[pl.BlockSpec((width...  6.19 us
    all_gather x1, waiting for transfers between devices, per_device(): up_rows = lax.all_gather(up_proj, 'tp', axis=1, tiled=True)  6.14 us
  transfers between devices with their start and end apart: 8, of which 4 were waited for; matrix products, arithmetic and copies ran while one was open for 7% of the time, Pallas kernels for 3%

profile of v1, /device:TPU:0, one launch (start us, length us, event | category | flops | bytes accessed | tf_op | source)
XLA Modules:
  0.0 215.1 jit_solution(10080610362124788344)
XLA Ops:
  6.6 0.7 all-gather.7.cloned.1.call-update
  7.3 0.7 all-gather.11.cloned.1.call-update
  8.1 0.7 all-gather.13.cloned.1.call-update
  8.8 0.9 slice.36
  9.7 2.4 %collective-permute-start = (bf16[256,3]{1,0:T(8,128)(2,1)S(1)}, bf16[256,3]{1,0:T(8,128)(2,1)S(1)}, u32[]{:S(2)}, u32[]{:S(2)}) collective-permute-start(bf16[256,3]{1,0:T(8,128)(2,1)S(1)} %slice.36), channel_id=1, source_target_pairs={{0,4},{4,8},{8,12},{12,16},{16,20},{20,24},{24,28},{1,5},{5,9},{9,... | collective-permute-start | bytes 4616 | tf_op jit(solution)/shard_map/ppermute | solution.py:32
  12.8 0.8 copy.32
  13.6 0.8 reshape.87.decay_ref
  14.6 0.7 pad.8.edge_ref
  15.3 6.2 %shard_map.163 = (f32[256,512]{1,0:T(8,128)}, f32[256,512]{1,0:T(8,128)}) custom-call(bf16[256,128]{1,0:T(8,128)(2,1)} %pad.8.edge_ref, bf16[256,512]{1,0:T(8,128)(2,1)} %input_ref.1, f32[4,64,4]{2,1,0:T(8,128)} %bitcast.78, bf16[4,64,64]{2,1,0:T(8,128)(2,1)} %rate_ref.1, bf16[4,64,64]{2,1,0:T(8,128)(2,1)} %inward_ref.1, f32[4,64,1]{2,1,0:T(8,128)} %reshape.87.decay_ref, ...), custom_call_target="tpu_custom_call" | custom-call | flops 52428800 | bytes 1572864 | tf_op jit(solution)/shard_map/pallas_call | solution.py:111
  21.5 1.1 slice.37
  22.5 19.6 %all-gather = f32[2048,1]{1,0:T(8,128)S(1)} all-gather(f32[256,1]{1,0:T(8,128)S(1)} %slice.37), channel_id=2, replica_groups=mesh['sp'=8,'tp'=4] {'sp'}, dimensions={0}, use_global_device_ids=true | all-gather | bytes 9216 | tf_op jit(solution)/shard_map/all_gather | solution.py:14
  42.2 0.3 reduce
  42.6 16.4 %all-gather.1 = f32[2048,1]{1,0:T(8,128)S(1)} all-gather(f32[256,1]{1,0:T(8,128)S(1)} %slice.38), channel_id=3, replica_groups=mesh['sp'=8,'tp'=4] {'sp'}, dimensions={0}, use_global_device_ids=true | all-gather | bytes 9216 | tf_op jit(solution)/shard_map/all_gather | solution.py:14
  59.0 0.3 reduce.1
  59.4 0.4 while.14
  59.8 1.0 copy_bitcast_fusion
  60.8 3.7 %all-to-all-start = ((bf16[256,4,128]{2,0,1:T(8,128)(2,1)}), bf16[256,4,128]{2,0,1:T(8,128)(2,1)S(1)}, u32[]{:S(2)}, u32[]{:S(2)}) async-start(bf16[256,4,128]{2,0,1:T(8,128)(2,1)} %copy_bitcast_fusion), calls=%async_computation | async-start | bytes 524288 | tf_op jit(solution)/shard_map/all_to_all | solution.py:239
  64.5 5.9 %all-to-all-done = bf16[256,4,128]{2,0,1:T(8,128)(2,1)S(1)} async-done(((bf16[256,4,128]{2,0,1:T(8,128)(2,1)}), bf16[256,4,128]{2,0,1:T(8,128)(2,1)S(1)}, u32[]{:S(2)}, u32[]{:S(2)}) %all-to-all-start) | async-done | bytes 262176 | tf_op jit(solution)/shard_map/all_to_all | solution.py:239
  70.4 3.1 %multiply_reduce_fusion.2 = (f32[128]{0:T(128)S(1)}, f32[128,2048]{1,0:T(8,128)S(1)}) fusion(bf16[1024,128]{1,0:T(8,128)(2,1)S(1)} %bitcast.75, bf16[1024,2048]{1,0:T(8,128)(2,1)} %all-gather.7.cloned.1.call-done), kind=kOutput, calls=%fused_computation.28 | convolution fusion | flops 537395072 | bytes 5505536 | tf_op jit(solution)/shard_map/dot_general | solution.py:241
  73.5 0.4 multiply_reduce_fusion.1
  74.5 20.8 %all_to_all.43 = bf16[8,16,2176]{2,1,0:T(8,128)(2,1)S(1)} all-to-all(bf16[8,16,2176]{2,1,0:T(8,128)(2,1)S(1)} %bitcast.76), channel_id=1, replica_groups=mesh['sp'=8,'tp'=4] {'sp'}, dimensions={0} | all-to-all | bytes 1114112 | tf_op jit(solution)/shard_map/all_to_all | solution.py:161
  95.5 6.1 %all-gather.11.cloned.1.call-done = bf16[1,512,2048]{2,1,0:T(8,128)(2,1)} async-done(((bf16[1,128,2048]{2,1,0:T(8,128)(2,1)}), bf16[1,512,2048]{2,1,0:T(8,128)(2,1)}) %all-gather.11.cloned.1.call-update) | async-done | bytes 2097168 | tf_op jit(solution)/shard_map/all_gather | solution.py:250
  101.6 2.6 %fusion.4 = f32[128,512]{1,0:T(8,128)S(1)} fusion(bf16[128,2048]{1,0:T(8,128)(2,1)S(1)} %collective-permute-done.1, bf16[1,512,2048]{2,1,0:T(8,128)(2,1)} %all-gather.11.cloned.1.call-done), kind=kOutput, calls=%fused_computation.10 | convolution fusion | flops 268435456 | bytes 2883584 | tf_op jit(solution)/shard_map/dot_general | solution.py:140
  104.2 34.4 %all-gather.13.cloned.1.call-done = bf16[1,512,2048]{2,1,0:T(8,128)(2,1)} async-done(((bf16[1,128,2048]{2,1,0:T(8,128)(2,1)}), bf16[1,512,2048]{2,1,0:T(8,128)(2,1)}) %all-gather.13.cloned.1.call-update) | async-done | bytes 2097168 | tf_op jit(solution)/shard_map/all_gather | solution.py:251
  138.7 36.9 %all-gather.9.cloned.1.call-done = bf16[1,512,2048]{2,1,0:T(8,128)(2,1)} async-done(((bf16[1,128,2048]{2,1,0:T(8,128)(2,1)}), bf16[1,512,2048]{2,1,0:T(8,128)(2,1)}) %all-gather.9.cloned.1.call-update) | async-done | bytes 2097168 | tf_op jit(solution)/shard_map/all_gather | solution.py:249
  175.6 4.6 %convolution_convert_fusion.1 = bf16[128,2048]{1,0:T(8,128)(2,1)} fusion(bf16[1,512,2048]{2,1,0:T(8,128)(2,1)} %all-gather.13.cloned.1.call-done, f32[128,512]{1,0:T(8,128)S(1)} %fusion.4, bf16[128,2048]{1,0:T(8,128)(2,1)} %copy-done.4, bf16[1,512,2048]{2,1,0:T(8,128)(2,1)} %all-gather.9.cloned.1.call-done), kind=kOutput, calls=%fused_computation.4 | convolution fusion | flops 537526272 | bytes 5505024 | tf_op jit(solution)/shard_map/dot_general | solution.py:142
  180.5 1.9 fusion.10
  182.4 0.8 copy-done.14
  183.2 3.7 %add_convert_fusion.1 = bf16[128,2048]{1,0:T(8,128)(2,1)S(1)} fusion(bf16[128,2048]{1,0:T(8,128)(2,1)} %copy-done.14, f32[128]{0:T(128)S(1)} %get-tuple-element.123, bf16[1,512,2048]{2,1,0:T(8,128)(2,1)} %all-gather.13.cloned.1.call-done, bf16[1,512,2048]{2,1,0:T(8,128)(2,1)} %all-gather.11.cloned.1.call-done, f32[128]{0:T(128)S(1)} %get-tuple-element.122, ...), kind=kOutput, calls=%fused_computation.24 | convolution fusion | flops 539099136 | bytes 6030336 | tf_op jit(solution)/shard_map/dot_general | solution.py:142
  187.0 20.0 %all_to_all.44 = bf16[8,16,2048]{2,1,0:T(8,128)(2,1)S(1)} all-to-all(bf16[8,16,2048]{2,1,0:T(8,128)(2,1)S(1)} %bitcast.77), channel_id=1, replica_groups=mesh['sp'=8,'tp'=4] {'sp'}, dimensions={0} | all-to-all | bytes 1048576 | tf_op jit(solution)/shard_map/all_to_all | solution.py:173
  206.9 0.4 multiply_reduce_fusion
  207.4 1.2 add_convert_fusion
  (84 shorter events, 2.2 us)
Async XLA Ops:
  6.5 5.6 %copy-start.12 = (bf16[4,256]{1,0:T(4,128)(2,1)S(1)}, bf16[4,256]{1,0:T(4,128)(2,1)}, u32[]{:S(2)}) copy-start(bf16[4,256]{1,0:T(4,128)(2,1)} %param.22) | copy-start | bytes 6148
  6.5 5.7 %copy-start.13 = (f32[256]{0:T(256)S(1)}, f32[256]{0:T(256)}, u32[]{:S(2)}) copy-start(f32[256]{0:T(256)} %param.25) | copy-start | bytes 3076
  6.5 5.7 %copy-start.15 = (s32[128,2]{0,1:T(2,128)S(1)}, s32[128,2]{0,1:T(2,128)}, u32[]{:S(2)}) copy-start(s32[128,2]{0,1:T(2,128)} %param.31) | copy-start | bytes 3076
  6.5 5.7 %copy-start.11 = (f32[128,2]{0,1:T(2,128)S(1)}, f32[128,2]{0,1:T(2,128)}, u32[]{:S(2)}) copy-start(f32[128,2]{0,1:T(2,128)} %param.32) | copy-start | bytes 3076
  6.5 63.9 %all-gather.7.cloned.1.call-start = ((), (), s32[]{:S(2)}) async-start(), calls=%async_computation.3 | async-start | bytes 5242880 | tf_op jit(solution)/shard_map/all_gather | solution.py:243
  7.3 94.3 %all-gather.11.cloned.1.call-start = ((), (), s32[]{:S(2)}) async-start(), calls=%async_computation.5 | async-start | bytes 2621440 | tf_op jit(solution)/shard_map/all_gather | solution.py:250
  8.0 130.7 %all-gather.13.cloned.1.call-start = ((), (), s32[]{:S(2)}) async-start(), calls=%async_computation.6 | async-start | bytes 2621440 | tf_op jit(solution)/shard_map/all_gather | solution.py:251
  8.8 166.8 %all-gather.9.cloned.1.call-start = ((), (), s32[]{:S(2)}) async-start(), calls=%async_computation.4 | async-start | bytes 2621440 | tf_op jit(solution)/shard_map/all_gather | solution.py:249
  9.7 4.8 %collective-permute-start = (bf16[256,3]{1,0:T(8,128)(2,1)S(1)}, bf16[256,3]{1,0:T(8,128)(2,1)S(1)}, u32[]{:S(2)}, u32[]{:S(2)}) collective-permute-start(bf16[256,3]{1,0:T(8,128)(2,1)S(1)} %slice.36), channel_id=1, source_target_pairs={{0,4},{4,8},{8,12},{12,16},{16,20},{20,24},{24,28},{1,5},{5,9},{9,... | collective-permute-start | bytes 4616 | tf_op jit(solution)/shard_map/ppermute | solution.py:32
  21.5 21.1 %copy-start.6 = (f32[256,512]{1,0:T(8,128)S(1)}, f32[256,512]{1,0:T(8,128)}, u32[]{:S(2)}) copy-start(f32[256,512]{1,0:T(8,128)} %get-tuple-element.101) | copy-start | bytes 1572868
  42.2 17.7 %copy-start.5 = (f32[256,512]{1,0:T(8,128)S(1)}, f32[256,512]{1,0:T(8,128)}, u32[]{:S(2)}) copy-start(f32[256,512]{1,0:T(8,128)} %get-tuple-element.102) | copy-start | bytes 1572868
  42.2 17.7 %copy-start.7 = (bf16[256,512]{1,0:T(8,128)(2,1)S(1)}, bf16[256,512]{1,0:T(8,128)(2,1)}, u32[]{:S(2)}) copy-start(bf16[256,512]{1,0:T(8,128)(2,1)} %param.21) | copy-start | bytes 786436
  60.8 9.6 %all-to-all-start = ((bf16[256,4,128]{2,0,1:T(8,128)(2,1)}), bf16[256,4,128]{2,0,1:T(8,128)(2,1)S(1)}, u32[]{:S(2)}, u32[]{:S(2)}) async-start(bf16[256,4,128]{2,0,1:T(8,128)(2,1)} %copy_bitcast_fusion), calls=%async_computation | async-start | bytes 524288 | tf_op jit(solution)/shard_map/all_to_all | solution.py:239
  70.4 3.1 %copy-start.2 = (bf16[128,2048]{1,0:T(8,128)(2,1)S(1)}, bf16[128,2048]{1,0:T(8,128)(2,1)}, u32[]{:S(2)}) copy-start(bf16[128,2048]{1,0:T(8,128)(2,1)} %param.19) | copy-start | bytes 1572868
  70.4 3.1 %copy-start.8 = (f32[2048]{0:T(1024)S(1)}, f32[2048]{0:T(1024)}, u32[]{:S(2)}) copy-start(f32[2048]{0:T(1024)} %param.28) | copy-start | bytes 24580
  70.4 3.5 %copy-start.9 = (f32[2048]{0:T(1024)S(1)}, f32[2048]{0:T(1024)}, u32[]{:S(2)}) copy-start(f32[2048]{0:T(1024)} %param.29) | copy-start | bytes 24580
  95.3 43.4 %copy-start.1 = (bf16[8,16,2176]{2,1,0:T(8,128)(2,1)}, bf16[8,16,2176]{2,1,0:T(8,128)(2,1)S(1)}, u32[]{:S(2)}) copy-start(bf16[8,16,2176]{2,1,0:T(8,128)(2,1)S(1)} %all_to_all.43) | copy-start | bytes 1671172
  95.4 6.3 %collective-permute-start.1 = (bf16[128,2048]{1,0:T(8,128)(2,1)S(1)}, bf16[128,2048]{1,0:T(8,128)(2,1)S(1)}, u32[]{:S(2)}, u32[]{:S(2)}) collective-permute-start(bf16[128,2048]{1,0:T(8,128)(2,1)S(1)} %slice.53), channel_id=1, source_target_pairs={{0,4},{4,0},{8,12},{12,8},{16,20},{20,16},{24,28},{28,24},{1,5},{5... | collective-permute-start | bytes 1572872 | tf_op jit(solution)/shard_map/ppermute | solution.py:163
  101.6 37.1 %copy-start.4 = (bf16[128,2048]{1,0:T(8,128)(2,1)}, bf16[128,2048]{1,0:T(8,128)(2,1)S(1)}, u32[]{:S(2)}) copy-start(bf16[128,2048]{1,0:T(8,128)(2,1)S(1)} %collective-permute-done.1) | copy-start | bytes 1572868
  175.6 4.9 %copy-start = (bf16[1,512,2048]{2,1,0:T(8,128)(2,1)S(1)}, bf16[1,512,2048]{2,1,0:T(8,128)(2,1)}, u32[]{:S(2)}) copy-start(bf16[1,512,2048]{2,1,0:T(8,128)(2,1)} %all-gather.9.cloned.1.call-done) | copy-start | bytes 6291460
  180.2 2.2 %collective-permute-start.2 = (bf16[128,2048]{1,0:T(8,128)(2,1)}, bf16[128,2048]{1,0:T(8,128)(2,1)S(1)}, u32[]{:S(2)}, u32[]{:S(2)}) collective-permute-start(bf16[128,2048]{1,0:T(8,128)(2,1)} %convolution_convert_fusion.1), channel_id=1, source_target_pairs={{0,4},{4,0},{8,12},{12,8},{16,20},{20,16},{24,28},{28,24},{1,5},{5... | collective-permute-start | bytes 1572872 | tf_op jit(solution)/shard_map/ppermute | solution.py:165
  182.4 0.8 copy-start.14
  186.9 20.4 %copy-start.3 = (bf16[128,2048]{1,0:T(8,128)(2,1)S(1)}, bf16[128,2048]{1,0:T(8,128)(2,1)}, u32[]{:S(2)}) copy-start(bf16[128,2048]{1,0:T(8,128)(2,1)} %param.19) | copy-start | bytes 1572868
  186.9 20.4 %copy-start.10 = (f32[2048]{0:T(1024)S(1)}, f32[2048]{0:T(1024)}, u32[]{:S(2)}) copy-start(f32[2048]{0:T(1024)} %param.30) | copy-start | bytes 24580
Sparse Core Ops, SparseCore 0:
  9.2 55.2 all-gather.6
  66.4 35.2 all-gather.10
  103.5 35.1 all-gather.12
  140.4 35.1 all-gather.8

commit v2 on v1

--- a/solution.py
+++ b/solution.py
@@ -257,6 +257,290 @@
     return (after_mix + normalized(moe, gain_post)).astype(jnp.bfloat16)
 
 
+def layer_kernel(
+    resid_ref, branch_ref, gatein_ref, taps_ref, rate_ref, inward_ref, decay_ref, extra_ref, outw_ref,
+    gmix_ref, gpre_ref, gpost_ref, ids_ref, rw_ref, gate_ref, up_ref, down_ref, out_ref,
+    edge, keep_s, state_s, carry, bo, br, owb, after_s, obuf, rows, gbuf, ubuf, dbuf, acc, res_send, res_recv, ret, back,
+    edge_sem, carry_sem, br_sem, ow_sem, fwd_sem, w_sem, disp_sem, swap_sem, ret_sem,
+):
+    f32, bf16 = jnp.float32, jnp.bfloat16
+    s, j = lax.axis_index("sp"), lax.axis_index("tp")
+    sp = lax.axis_size("sp")
+    c = s % 2
+    partner = s + 1 - 2 * c
+    jx, jy = j % 2, j // 2
+
+    def tp_peer(k):
+        x = 1 - jx if k % 2 else jx
+        y = 1 - jy if k // 2 else jy
+        return y * 2 + x
+
+    def later(k):
+        return (s + k) % sp
+
+    def earlier(k):
+        return (s + sp - k) % sp
+
+    sent = []
+
+    def send(src, dst, sem, at, device):
+        copy = pltpu.make_async_remote_copy(
+            src_ref=src, dst_ref=dst, send_sem=sem.at[0, at], recv_sem=sem.at[1, at],
+            device_id=device, device_id_type=pl.DeviceIdType.MESH,
+        )
+        copy.start()
+        sent.append(copy)
+        return copy
+
+    barrier = pltpu.get_barrier_semaphore()
+    for k in range(1, 4):
+        pl.semaphore_signal(barrier, inc=1, device_id=(s, tp_peer(k)), device_id_type=pl.DeviceIdType.MESH)
+    for k in range(1, sp):
+        pl.semaphore_signal(barrier, inc=1, device_id=(later(k), j), device_id_type=pl.DeviceIdType.MESH)
+    pl.semaphore_wait(barrier, sp + 2)
+
+    channels, positions = branch_ref.shape
+    tile = 128
+    edge_copy = send(branch_ref.at[:, positions - tile :], edge, edge_sem, 0, (later(1), j))
+    half = channels // 2
+    ow_in = {}
+    for k in (3, 1, 2):
+        ow_in[k] = send(outw_ref.at[pl.ds(c * half, half)], owb.at[k, c], ow_sem, k, (s, tp_peer(k)))
+    w_in = {}
+    for m, (ref, buf) in enumerate(((gate_ref, gbuf), (up_ref, ubuf), (down_ref, dbuf))):
+        for k in (1, 2, 3):
+            w_in[m, k] = send(ref.at[0], buf.at[k], w_sem, m * 4 + k, (s, tp_peer(k)))
+
+    edge_copy.wait_recv()
+    blocks, width = rate_ref.shape[0], rate_ref.shape[1]
+    count = taps_ref.shape[2]
+    started = jnp.where(s > 0, 1.0, 0.0)
+
+    def scan_block(n, none):
+        at = pl.ds(pl.multiple_of(n * width, width), width)
+        taps = taps_ref[n]
+        here = branch_ref[at, :].astype(f32)
+        padded = jnp.concatenate([edge[at, :].astype(f32) * started, here], axis=1)
+        convolved = taps[:, count - 1 : count] * here
+        for step in range(1, count):
+            moved = pltpu.roll(padded, step, 1)[:, tile:]
+            convolved = convolved + taps[:, count - 1 - step : count - step] * moved
+        stacked = jnp.concatenate(split_three(convolved), axis=0)
+
+        def gate(weight):
+            return jax.nn.sigmoid(
+                lax.dot_general(
+                    jnp.concatenate([weight] * 3, axis=0), stacked,
+                    (((0,), (0,)), ((), ())), preferred_element_type=f32,
+                )
+            )
+
+        log_keep = decay_ref[n] * gate(rate_ref[n]) + extra_ref[...]
+        state = jnp.sqrt(one_minus_exp(2.0 * log_keep)) * gate(inward_ref[n]) * convolved
+        keep = jnp.exp(log_keep)
+        lane = lax.broadcasted_iota(jnp.int32, keep.shape, 1)
+        distance = 1
+        while distance < positions:
+            state = keep * shifted(state, 0.0, distance, lane) + state
+            keep = keep * shifted(keep, 1.0, distance, lane)
+            distance *= 2
+        keep_s[at, :] = keep
+        state_s[at, :] = state
+        return none
+
+    lax.fori_loop(0, blocks, scan_block, 0)
+    carry[0, 0:1, :] = keep_s[:, positions - tile :].T[tile - 1 : tile, :]
+    carry[0, 1:2, :] = state_s[:, positions - tile :].T[tile - 1 : tile, :]
+    carry_in_copies = {}
+    for k in range(1, sp):
+        carry_in_copies[k] = send(carry.at[0], carry.at[k], carry_sem, k, (later(k), j))
+    entering = jnp.zeros((1, channels), f32)
+    for k in range(sp - 1, 0, -1):
+        carry_in_copies[k].wait_recv()
+        entering = jnp.where(k <= s, carry[k, 0:1, :] * entering + carry[k, 1:2, :], entering)
+    entering = jnp.broadcast_to(entering, (tile, channels)).T[:, 0:1]
+    tokens = resid_ref.shape[0]
+    for q in range(4):
+        cols = slice(q * tokens, (q + 1) * tokens)
+        hidden = state_s[:, cols] + keep_s[:, cols] * entering
+        bo[q] = (hidden * jax.nn.gelu(gatein_ref[:, cols].astype(f32), approximate=True)).astype(bf16)
+    br_in = {}
+    for k in (3, 1, 2):
+        br_in[k] = send(bo.at[tp_peer(k)], br.at[k], br_sem, k, (s, tp_peer(k)))
+    br[0] = bo[j]
+    owb[0, 0] = outw_ref[0:half, :]
+    owb[0, 1] = outw_ref[half:, :]
+    fwd = []
+    for k in (3, 1, 2):
+        ow_in[k].wait_recv()
+        fwd.append(send(owb.at[k, c], owb.at[k, c], fwd_sem, k, (partner, j)))
+
+    ids = ids_ref[...]
+    first_id = ids[:, 0:1]
+    group = first_id >> 1
+    odd = first_id & 1
+    lane = lax.broadcasted_iota(jnp.int32, (tokens, tokens), 1)
+    sub = lax.broadcasted_iota(jnp.int32, (tokens, tokens), 0)
+    member = jnp.where(lane == group, 1.0, 0.0)
+    below = jnp.where(sub > lane, 1.0, 0.0).astype(bf16)
+    prefix = jnp.dot(below, member.astype(bf16), preferred_element_type=f32)
+    rank = jnp.sum(prefix * member, axis=1, keepdims=True)
+    cap = tokens // (sp // 2)
+    slot = group.astype(f32) * cap + rank
+    place = jnp.where(slot == lane.astype(f32), 1.0, 0.0).astype(bf16)
+    rw = rw_ref[...]
+    w_even = jnp.where(odd == 0, rw[:, 0:1], rw[:, 1:2])
+    w_odd = jnp.where(odd == 0, rw[:, 1:2], rw[:, 0:1])
+    extra = jnp.zeros((tokens, tile), f32)
+    lane_e = lax.broadcasted_iota(jnp.int32, (tokens, tile), 1)
+    for at, piece in enumerate(split_three(w_even) + split_three(w_odd)):
+        extra = jnp.where(lane_e == at, piece.astype(f32), extra)
+
+    for k in (3, 1, 2):
+        br_in[k].wait_recv()
+    for copy in fwd:
+        copy.wait_recv()
+    features = resid_ref.shape[1]
+    step = 512
+
+    def mix_tile(t, none):
+        cols = pl.ds(pl.multiple_of(t * step, step), step)
+        total = jnp.zeros((tokens, step), f32)
+        for k in range(4):
+            for h in range(2):
+                total = total + lax.dot_general(
+                    br[k, h * half : (h + 1) * half, :], owb[k, h, :, cols],
+                    (((0,), (0,)), ((), ())), preferred_element_type=f32,
+                )
+        after_s[:, cols] = total
+        return none
+
+    lax.fori_loop(0, features // step, mix_tile, 0)
+    after_s[...] = resid_ref[...].astype(f32) + normalized(after_s[...], gmix_ref[...])
+    acc_rows = normalized(after_s[...], gpre_ref[...]).astype(bf16)
+    res_send[...] = acc_rows
+    each = tokens // sp
+
+    def place_rows(values):
+        return lax.dot_general(place, values, (((0,), (0,)), ((), ())), preferred_element_type=f32).astype(bf16)
+
+    def place_tile(t, none):
+        cols = pl.ds(pl.multiple_of(t * step, step), step)
+        obuf[:, :, cols] = place_rows(res_send[:, cols]).reshape(sp, each, step)
+        return none
+
+    lax.fori_loop(0, features // step, place_tile, 0)
+    obuf[:, :, features:] = place_rows(extra.astype(bf16)).reshape(sp, each, tile)
+    disp = []
+    for k in range(sp - 1, 0, -1):
+        disp.append(send(obuf.at[later(k)], rows.at[k], disp_sem, k, (later(k), j)))
+    rows[0] = obuf[s]
+    for copy in disp:
+        copy.wait_recv()
+    swap = send(rows.at[0:sp], rows.at[sp : 2 * sp], swap_sem, 0, (partner, j))
+    swap.wait_recv()
+
+    contract = (((1,), (1,)), ((), ()))
+    for k in range(4):
+        if k:
+            w_in[0, k].wait_recv()
+            w_in[1, k].wait_recv()
+        gate_w = gbuf.at[k] if k else gate_ref.at[0]
+        up_w = ubuf.at[k] if k else up_ref.at[0]
+        down_w = dbuf.at[k] if k else down_ref.at[0]
+        arrived = rows[:, :, 0:features].reshape(2 * tokens, features)
+        gate_vals = lax.dot_general(arrived, gate_w[...], contract, preferred_element_type=f32)
+        up_vals = lax.dot_general(arrived, up_w[...], contract, preferred_element_type=f32)
+        hidden = (jax.nn.silu(gate_vals) * up_vals).astype(bf16)
+        if k:
+            w_in[2, k].wait_recv()
+
+        def down_tile(t, none):
+            cols = pl.ds(pl.multiple_of(t * step, step), step)
+            part = jnp.dot(hidden, down_w[:, cols], preferred_element_type=f32)
+            acc[:, cols] = part if k == 0 else acc[:, cols] + part
+            return none
+
+        lax.fori_loop(0, features // step, down_tile, 0)
+    res_send[...] = acc[tokens:, :].astype(bf16)
+    result = send(res_send, res_recv, swap_sem, 1, (partner, j))
+    scales = rows[0:sp, :, features:].reshape(tokens, tile).astype(f32)
+    s_even = jnp.sum(jnp.where(lane_e < 3, scales, 0.0), axis=1, keepdims=True)
+    s_odd = jnp.sum(jnp.where((lane_e >= 3) & (lane_e < 6), scales, 0.0), axis=1, keepdims=True)
+    own_scale = jnp.where(c == 0, s_even, s_odd)
+    other_scale = jnp.where(c == 0, s_odd, s_even)
+    own = own_scale * acc[0:tokens, :].astype(bf16).astype(f32)
+    result.wait_recv()
+    ret[...] = (own + other_scale * res_recv[...].astype(f32)).astype(bf16).reshape(sp, each, features)
+    home = []
+    for k in range(sp - 1, 0, -1):
+        home.append(send(ret.at[k], back.at[s], ret_sem, k, (earlier(k), j)))
+    back[s] = ret[0]
+    for copy in home:
+        copy.wait_recv()
+
+    def gather_tile(t, none):
+        cols = pl.ds(pl.multiple_of(t * step, step), step)
+        acc[0:tokens, cols] = jnp.dot(place, back[:, :, cols].reshape(tokens, step), preferred_element_type=f32)
+        return none
+
+    lax.fori_loop(0, features // step, gather_tile, 0)
+    out_ref[...] = (after_s[...] + normalized(acc[0:tokens, :], gpost_ref[...])).astype(out_ref.dtype)
+    for copy in sent:
+        copy.wait_send()
+
+
+def fused_layer(
+    resid, branch_input, gate_in, conv_taps, rate_weight, input_weight, decay_base, decay_extra, out_weight,
+    gain_mix, gain_pre, gain_post, expert_ids, route_weight, gate_proj, up_proj, down_proj,
+):
+    channels, positions = branch_input.shape
+    blocks, width = rate_weight.shape[:2]
+    tokens, features = resid.shape
+    sp = lax.axis_size("sp")
+    hid = gate_proj.shape[1]
+    each = tokens // sp
+    f32, bf16 = jnp.float32, jnp.bfloat16
+    taps = conv_taps.astype(f32).T.reshape(blocks, width, conv_taps.shape[0])
+    decay_rate = (-gate_power * jax.nn.softplus(-decay_base)).reshape(blocks, width, 1)
+    sems = lambda n: pltpu.SemaphoreType.DMA((2, n))
+    vm = pltpu.VMEM
+    return pl.pallas_call(
+        layer_kernel,
+        out_shape=jax.ShapeDtypeStruct((tokens, features), bf16),
+        in_specs=[pl.BlockSpec(memory_space=pltpu.VMEM)] * 17,
+        out_specs=pl.BlockSpec(memory_space=pltpu.VMEM),
+        scratch_shapes=[
+            vm((channels, 128), bf16),
+            vm((channels, positions), f32),
+            vm((channels, positions), f32),
+            vm((sp, 8, channels), f32),
+            vm((4, channels, tokens), bf16),
+            vm((4, channels, tokens), bf16),
+            vm((4, 2, channels // 2, features), bf16),
+            vm((tokens, features), f32),
+            vm((sp, each, features + 128), bf16),
+            vm((2 * sp, each, features + 128), bf16),
+            vm((4, hid, features), bf16),
+            vm((4, hid, features), bf16),
+            vm((4, hid, features), bf16),
+            vm((2 * tokens, features), f32),
+            vm((tokens, features), bf16),
+            vm((tokens, features), bf16),
+            vm((sp, each, features), bf16),
+            vm((sp, each, features), bf16),
+            sems(1), sems(sp), sems(4), sems(4), sems(4), sems(12), sems(sp), sems(2), sems(sp),
+        ],
+        compiler_params=pltpu.CompilerParams(
+            collective_id=0, has_side_effects=True, vmem_limit_bytes=60 * 1024 * 1024
+        ),
+    )(
+        resid, branch_input, gate_in, taps, rate_weight, input_weight, decay_rate,
+        decay_extra.reshape(1, positions), out_weight, gain_mix.reshape(1, -1), gain_pre.reshape(1, -1),
+        gain_post.reshape(1, -1), expert_ids, route_weight, gate_proj, up_proj, down_proj,
+    )
+
+
 def solution(mesh):
     in_specs = (
         P(("sp", "tp"), None),
@@ -278,6 +562,7 @@
         P("sp", "tp", None),
     )
     out_specs = P(("sp", "tp"), None)
+    paired = mesh.shape["tp"] == 4 and mesh.shape["sp"] == 2 * expert_groups
     return jax.shard_map(
-        per_device, mesh=mesh, in_specs=in_specs, out_specs=out_specs, check_vma=False
-    )
+        fused_layer if paired else per_device, mesh=mesh, in_specs=in_specs, out_specs=out_specs, check_vma=False
+    )

time: 216 us -> 147 us (0.68)
  Pallas kernels: 6.19 us -> 139 us
  waiting for transfers between devices: 85.4 us -> 0 us
  blocking collectives: 76.8 us -> 0 us
  matrix products: 16.6 us -> 0 us
  between operations: 13.5 us -> 0.03 us
  starting transfers between devices: 6.34 us -> 0 us
  other arithmetic: 4.45 us -> 0.02 us
    pallas_call x1, Pallas kernels: 6.19 us -> 139 us  [fused_layer(): pl.pallas_call(layer_kernel, out_shape=jax.ShapeDtypeStruct((tokens, feat...]
    all_gather x4 -> x0, waiting for transfers between devices: 77.5 us -> none  [the longest x1 36.9 us: per_device(): gate_rows = lax.all_gather(gate_proj, 'tp', axis=1, tiled=True)]
    all_to_all x2 -> x0, blocking collectives: 40.8 us -> none  [the longest x1 20.8 us: paired_moe(): lax.all_to_all(outgoing, 'sp', split_axis=0, concat_axis=0, tiled=True)]
    all_gather x2 -> x0, blocking collectives: 36.1 us -> none  [entering_2(): everything = jax.tree.map(lambda part: lax.all_gather(part, axis), array)]
    dot_general x7 -> x0, matrix products: 16.6 us -> none  [the longest x2 8.35 us: expert_mlp(): jnp.dot(hidden, down_rows, preferred_element_type=jnp.float32)]
    all_to_all x1 -> x0, waiting for transfers between devices: 5.86 us -> none  [per_device(): lax.all_to_all(branch_out, 'tp', split_axis=1, concat_axis=0, tiled=True)]
    unnamed x32 -> x11, local copies, waits for them, and re-layouts: 0.85 us -> 4.68 us
    all_to_all x1 -> x0, starting transfers between devices: 3.72 us -> none  [per_device(): lax.all_to_all(branch_out, 'tp', split_axis=1, concat_axis=0, tiled=True)]
  transfers between devices with their start and end apart: 8 -> 0, of which waited for: 4 -> 0; matrix products, arithmetic and copies ran while one was open for 7% -> 0% of each run, Pallas kernels for 3% -> 0%
where the time goes in v2:
time: 147 us; the launch traced here: 145 us
  Pallas kernels  139 us (95%)
  local copies, waits for them, and re-layouts  6.33 us (4%)
    pallas_call x1, Pallas kernels, fused_layer(): pl.pallas_call(layer_kernel, out_shape=jax.ShapeDtypeStruct((tokens, feat...  139 us
    unnamed x11, local copies, waits for them, and re-layouts  4.68 us

profile of v2, /device:TPU:0, one launch (start us, length us, event | category | flops | bytes accessed | tf_op | source)
XLA Modules:
  0.0 145.0 jit_solution(11693144089149832498)
XLA Ops:
  0.0 0.0 copy-start.3
  0.0 0.0 copy-start
  0.0 0.7 copy-done.3
  0.7 0.0 copy-done
  0.7 0.0 copy-start.1
  0.7 0.7 copy-done.1
  1.4 0.0 copy-start.2
  1.4 0.7 copy.23.ids_ref
  2.1 0.0 copy-done.2
  2.1 0.7 copy.24.rw_ref
  2.8 0.8 copy.21
  3.6 0.8 reshape.30.decay_ref
  4.5 138.7 %shard_map.163 = bf16[128,2048]{1,0:T(8,128)(2,1)} custom-call(bf16[128,2048]{1,0:T(8,128)(2,1)} %resid_ref.1, bf16[256,512]{1,0:T(8,128)(2,1)} %branch_ref.1, bf16[256,512]{1,0:T(8,128)(2,1)} %gatein_ref.1, f32[4,64,4]{2,1,0:T(8,128)} %bitcast.7, bf16[4,64,64]{2,1,0:T(8,128)(2,1)} %rate_ref.1, bf16[4,64,64]{2,1,0:T(8,128)(2,1)} %inward_ref.1, ...), custom_call_target="tpu_custom_call" | custom-call | tf_op jit(solution)/shard_map/pallas_call | solution.py:508
  143.2 1.9 %copy.26 = bf16[128,2048]{1,0:T(8,128)(2,1)} copy(bf16[128,2048]{1,0:T(8,128)(2,1)} %shard_map.163) | data formatting | bytes 1048576
  (2 shorter events, 0.0 us)
Async XLA Ops:
  0.0 0.7 copy-start.3
  0.0 0.7 copy-start
  0.7 0.7 copy-start.1
  1.4 0.7 copy-start.2

commit v3 on v2

--- a/solution.py
+++ b/solution.py
@@ -307,9 +307,21 @@
     for k in (3, 1, 2):
         ow_in[k] = send(outw_ref.at[pl.ds(c * half, half)], owb.at[k, c], ow_sem, k, (s, tp_peer(k)))
     w_in = {}
-    for m, (ref, buf) in enumerate(((gate_ref, gbuf), (up_ref, ubuf), (down_ref, dbuf))):
-        for k in (1, 2, 3):
+    weights = ((gate_ref, gbuf), (up_ref, ubuf), (down_ref, dbuf))
+    hid_half = gate_ref.shape[1] // 2
+
+    def send_weight(m):
+        ref, buf = weights[m]
+        for k in (1, 2):
             w_in[m, k] = send(ref.at[0], buf.at[k], w_sem, m * 4 + k, (s, tp_peer(k)))
+
+    def relay_weight(m):
+        buf = weights[m][1]
+        upper, lower = pl.ds(0, hid_half), pl.ds(hid_half, hid_half)
+        w_in[m, 1].wait_recv()
+        w_in[m, 3] = send(buf.at[1, upper], buf.at[3, upper], w_sem, m * 4 + 3, (s, tp_peer(2)))
+        w_in[m, 2].wait_recv()
+        w_in[m, 0] = send(buf.at[2, lower], buf.at[3, lower], w_sem, m * 4, (s, tp_peer(1)))
 
     edge_copy.wait_recv()
     blocks, width = rate_ref.shape[0], rate_ref.shape[1]
@@ -367,6 +379,8 @@
     br_in = {}
     for k in (3, 1, 2):
         br_in[k] = send(bo.at[tp_peer(k)], br.at[k], br_sem, k, (s, tp_peer(k)))
+    send_weight(0)
+    send_weight(1)
     br[0] = bo[j]
     owb[0, 0] = outw_ref[0:half, :]
     owb[0, 1] = outw_ref[half:, :]
@@ -435,29 +449,38 @@
     for k in range(sp - 1, 0, -1):
         disp.append(send(obuf.at[later(k)], rows.at[k], disp_sem, k, (later(k), j)))
     rows[0] = obuf[s]
+    relay_weight(0)
+    relay_weight(1)
+    send_weight(2)
     for copy in disp:
         copy.wait_recv()
     swap = send(rows.at[0:sp], rows.at[sp : 2 * sp], swap_sem, 0, (partner, j))
     swap.wait_recv()
 
     contract = (((1,), (1,)), ((), ()))
+    hiddens = []
     for k in range(4):
-        if k:
-            w_in[0, k].wait_recv()
-            w_in[1, k].wait_recv()
+        if k == 3:
+            for at in (3, 0):
+                w_in[0, at].wait_recv()
+                w_in[1, at].wait_recv()
         gate_w = gbuf.at[k] if k else gate_ref.at[0]
         up_w = ubuf.at[k] if k else up_ref.at[0]
-        down_w = dbuf.at[k] if k else down_ref.at[0]
         arrived = rows[:, :, 0:features].reshape(2 * tokens, features)
         gate_vals = lax.dot_general(arrived, gate_w[...], contract, preferred_element_type=f32)
         up_vals = lax.dot_general(arrived, up_w[...], contract, preferred_element_type=f32)
-        hidden = (jax.nn.silu(gate_vals) * up_vals).astype(bf16)
-        if k:
-            w_in[2, k].wait_recv()
+        hiddens.append((jax.nn.silu(gate_vals) * up_vals).astype(bf16))
+    for k in range(4):
+        if k == 1:
+            relay_weight(2)
+        if k == 3:
+            w_in[2, 3].wait_recv()
+            w_in[2, 0].wait_recv()
+        down_w = dbuf.at[k] if k else down_ref.at[0]
 
         def down_tile(t, none):
             cols = pl.ds(pl.multiple_of(t * step, step), step)
-            part = jnp.dot(hidden, down_w[:, cols], preferred_element_type=f32)
+            part = jnp.dot(hiddens[k], down_w[:, cols], preferred_element_type=f32)
             acc[:, cols] = part if k == 0 else acc[:, cols] + part
             return none
 

time: 147 us -> 110 us (0.75)
  the two profiles are of different devices: /device:TPU:0 before, /device:TPU:25 now
where the time goes in v3:
time: 110 us
  Pallas kernels  103 us (94%)
  local copies, waits for them, and re-layouts  6.33 us (6%)
    pallas_call x1, Pallas kernels, fused_layer(): pl.pallas_call(layer_kernel, out_shape=jax.ShapeDtypeStruct((tokens, feat...  103 us
    unnamed x11, local copies, waits for them, and re-layouts  4.68 us

profile of v3, /device:TPU:25, one launch (start us, length us, event | category | flops | bytes accessed | tf_op | source)
XLA Modules:
  0.0 109.8 jit_solution(11162789791389351835)
XLA Ops:
  0.0 0.0 copy-start.3
  0.0 0.0 copy-start
  0.0 0.7 copy-done.3
  0.7 0.0 copy-done
  0.7 0.0 copy-start.1
  0.7 0.7 copy-done.1
  1.4 0.0 copy-start.2
  1.4 0.7 copy.23.ids_ref
  2.1 0.0 copy-done.2
  2.1 0.7 copy.24.rw_ref
  2.8 0.8 copy.21
  3.6 0.8 reshape.30.decay_ref
  4.5 103.4 %shard_map.163 = bf16[128,2048]{1,0:T(8,128)(2,1)} custom-call(bf16[128,2048]{1,0:T(8,128)(2,1)} %resid_ref.1, bf16[256,512]{1,0:T(8,128)(2,1)} %branch_ref.1, bf16[256,512]{1,0:T(8,128)(2,1)} %gatein_ref.1, f32[4,64,4]{2,1,0:T(8,128)} %bitcast.7, bf16[4,64,64]{2,1,0:T(8,128)(2,1)} %rate_ref.1, bf16[4,64,64]{2,1,0:T(8,128)(2,1)} %inward_ref.1, ...), custom_call_target="tpu_custom_call" | custom-call | tf_op jit(solution)/shard_map/pallas_call | solution.py:531
  107.9 1.9 %copy.26 = bf16[128,2048]{1,0:T(8,128)(2,1)} copy(bf16[128,2048]{1,0:T(8,128)(2,1)} %shard_map.163) | data formatting | bytes 1048576
  (2 shorter events, 0.0 us)
Async XLA Ops:
  0.0 0.7 copy-start.3
  0.0 0.7 copy-start
  0.7 0.7 copy-start.1
  1.4 0.7 copy-start.2
